TPU v7x, 32 devices: a whole 2x2x4 slice. The times are simulated.
32 devices in a mesh: ep: 8 (over z, x), tp: 4 (over y, core).
Axes of the slice: x: 2, y: 2, z: 4, core: 2. Of those that a mesh axis runs over, the one named last changes fastest.
Arguments:
- tokens: bfloat16 [32, 2048], P('ep'), may hold values from -6 to 6
- norm_gain: bfloat16 [2048], replicated, may hold values from 0.099609375 to 1.8984375
- in_weight: bfloat16 [2048, 1024], P(None, 'tp'), may hold values from -0.125 to 0.125
- decay_rate: float32 [64, 64], P('tp'), may hold values from 0.05 to 1
- frequency: float32 [64, 64], P('tp'), may hold values from -3 to 3
- log_step: float32 [64], P('tp'), may hold values from -2.3 to 0.7
- input_real: float32 [64, 64, 16], P('tp'), may hold values from -1.75 to 1.75
- input_imag: float32 [64, 64, 16], P('tp'), may hold values from -1.75 to 1.75
- output_real: float32 [64, 16, 64], P('tp'), may hold values from -0.5 to 0.5
- output_imag: float32 [64, 16, 64], P('tp'), may hold values from -0.5 to 0.5
- skip_gain: float32 [1024], P('tp'), may hold values from -3 to 3
- state_real: float32 [32, 64, 64], P('ep', 'tp'), may hold values from -6 to 6
- state_imag: float32 [32, 64, 64], P('ep', 'tp'), may hold values from -6 to 6
- out_weight: bfloat16 [1024, 2048], P('tp'), may hold values from -0.1875 to 0.1875
- ffn_gain: bfloat16 [2048], replicated, may hold values from 0.099609375 to 1.8984375
- expert_ids: int32 [32, 2], replicated, may hold values from 0 to 7, all different within a row; in each aligned block of 4 rows (0 to 3, 4 to 7, ...) at most 2 rows name the same one
- route_weights: float32 [32, 2], P('ep'), may hold values from 0.2 to 1
- gate_weight: bfloat16 [2048, 65536], P(None, ('ep', 'tp')), may hold values from -0.125 to 0.125
- up_weight: bfloat16 [2048, 65536], P(None, ('ep', 'tp')), may hold values from -0.125 to 0.125
- down_weight: bfloat16 [65536, 2048], P('ep', 'tp'), may hold values from -0.0625 to 0.0625
Outputs:
- mixed: bfloat16 [32, 2048], P('ep', 'tp')
- new_real: float32 [32, 64, 64], P('ep', 'tp')
- new_imag: float32 [32, 64, 64], P('ep', 'tp')
Inputs may be any that keep to these rules, and one draw needn't show every extreme that they name: `expert_ids`: the 2 experts of a row differ. In each aligned block of 4 rows (the rows of one index of ep) no expert is named by more than 2 rows, and in some blocks one expert is named by exactly 2 rows.
All inputs are finite; a program needn't handle non-finite values.
Results may differ from a plain program's by a relative error of at most 0.007.
Values may be sent and summed in bfloat16 or wider, within the bound.
No kernel may reach another device: no remote copies, remote signals or barrier semaphores. Data moves between devices by JAX's collectives and lax.ppermute only.
A program may use at most 64 MiB of HBM per device.

v0:
```python
import jax
import jax.numpy as jnp
from jax import lax
from jax.sharding import PartitionSpec as P

EXPERTS = 8


EPSILON = 1e-06


def rms_scale(values, gain):
    floats = values.astype(jnp.float32)
    return (
        floats
        * lax.rsqrt(jnp.mean(floats * floats, axis=-1, keepdims=True) + EPSILON)
        * gain.astype(jnp.float32)
    )


def discretize(decay_rate, frequency, log_step, input_real, input_imag):
    step_size = jnp.exp(log_step)[:, None]
    lam_real = -decay_rate
    magnitude = jnp.exp(lam_real * step_size)
    turned = frequency * step_size
    bar_real = magnitude * jnp.cos(turned)
    bar_imag = magnitude * jnp.sin(turned)
    denom = lam_real * lam_real + frequency * frequency
    minus_one = bar_real - 1.0
    factor_real = (minus_one * lam_real + bar_imag * frequency) / denom
    factor_imag = (bar_imag * lam_real - minus_one * frequency) / denom
    b_real = factor_real[..., None] * input_real - factor_imag[..., None] * input_imag
    b_imag = factor_real[..., None] * input_imag + factor_imag[..., None] * input_real
    return (bar_real, bar_imag, b_real, b_imag)


def state_update(
    projected,
    state_real,
    state_imag,
    decay_rate,
    frequency,
    log_step,
    input_real,
    input_imag,
    output_real,
    output_imag,
    skip_gain,
):
    bar_real, bar_imag, b_real, b_imag = discretize(
        decay_rate, frequency, log_step, input_real, input_imag
    )
    count, groups, _ = state_real.shape
    high = lax.Precision.HIGHEST
    grouped = projected.astype(jnp.float32).reshape(count, groups, -1)
    drive_real = jnp.einsum("sgp,gnp->sgn", grouped, b_real, precision=high)
    drive_imag = jnp.einsum("sgp,gnp->sgn", grouped, b_imag, precision=high)
    new_real = bar_real * state_real - bar_imag * state_imag + drive_real
    new_imag = bar_real * state_imag + bar_imag * state_real + drive_imag
    readout = jnp.einsum("sgn,gpn->sgp", new_real, output_real, precision=high) - jnp.einsum(
        "sgn,gpn->sgp", new_imag, output_imag, precision=high
    )
    readout = readout.reshape(count, -1) + skip_gain * grouped.reshape(count, -1)
    return (jax.nn.gelu(readout).astype(jnp.bfloat16), new_real, new_imag)


def slot_table(own_ids, own_weights, slot_count):
    expert_range = jnp.arange(EXPERTS, dtype=jnp.int32)
    onehot = (own_ids[:, :, None] == expert_range).astype(jnp.int32)
    flat = onehot.reshape(-1, EXPERTS)
    before = (jnp.cumsum(flat, axis=0) - flat).reshape(onehot.shape)
    slots = jnp.arange(slot_count, dtype=jnp.int32)
    match = (before[..., None] == slots) & (onehot[..., None] > 0)
    table = jnp.sum(jnp.where(match, own_weights[:, :, None, None], 0.0), axis=1)
    return jnp.transpose(table, (1, 2, 0))


def shards(
    tokens,
    norm_gain,
    in_weight,
    decay_rate,
    frequency,
    log_step,
    input_real,
    input_imag,
    output_real,
    output_imag,
    skip_gain,
    state_real,
    state_imag,
    out_weight,
    ffn_gain,
    expert_ids,
    route_weights,
    gate_weight,
    up_weight,
    down_weight,
):
    normed_in = rms_scale(tokens, norm_gain).astype(jnp.bfloat16)
    projected = jnp.dot(normed_in, in_weight, preferred_element_type=jnp.float32).astype(
        jnp.bfloat16
    )
    activated, new_real, new_imag = state_update(
        projected,
        state_real,
        state_imag,
        decay_rate,
        frequency,
        log_step,
        input_real,
        input_imag,
        output_real,
        output_imag,
        skip_gain,
    )
    delta = lax.psum(jnp.dot(activated, out_weight, preferred_element_type=jnp.float32), "tp")
    hidden_state = (tokens.astype(jnp.float32) + delta).astype(jnp.bfloat16)
    normed = rms_scale(hidden_state, ffn_gain).astype(jnp.bfloat16)
    seq_count, width = normed.shape
    slot_count = seq_count // 2
    group_span = lax.axis_size("ep") // EXPERTS
    my_index = lax.axis_index("ep")
    own_ids = lax.dynamic_slice_in_dim(expert_ids, my_index * seq_count, seq_count, 0)
    unit_weights = jnp.ones(own_ids.shape, jnp.float32)
    select = slot_table(own_ids, unit_weights, slot_count)
    outgoing = jnp.einsum(
        "xcs,sd->xcd", select.astype(jnp.bfloat16), normed, preferred_element_type=jnp.float32
    ).astype(jnp.bfloat16)
    received = lax.all_to_all(
        jnp.repeat(outgoing, group_span, axis=0), "ep", split_axis=0, concat_axis=0, tiled=True
    )
    slot_rows = received.reshape(-1, width)
    gate_pre = jnp.dot(slot_rows, gate_weight, preferred_element_type=jnp.float32)
    up_pre = jnp.dot(slot_rows, up_weight, preferred_element_type=jnp.float32)
    hidden = (jax.nn.silu(gate_pre) * up_pre).astype(jnp.bfloat16)
    quarter = down_weight.shape[1]
    partial_out = jnp.dot(
        lax.all_gather(hidden, "tp", axis=1, tiled=True),
        down_weight,
        preferred_element_type=jnp.float32,
    )
    rounded = partial_out.astype(jnp.bfloat16).reshape(-1, slot_count, quarter)
    returned = lax.all_to_all(rounded, "ep", split_axis=0, concat_axis=0, tiled=True)
    summed = (
        returned.astype(jnp.float32).reshape(EXPERTS, group_span, slot_count, quarter).sum(axis=1)
    )
    weight_table = slot_table(own_ids, route_weights, slot_count)
    routed = jnp.einsum("xcs,xcd->sd", weight_table, summed, precision=lax.Precision.HIGHEST)
    residual = lax.dynamic_slice_in_dim(hidden_state, lax.axis_index("tp") * quarter, quarter, 1)
    mixed = (residual.astype(jnp.float32) + routed).astype(jnp.bfloat16)
    return (mixed, new_real, new_imag)


def solution(mesh):
    in_specs = (
        P("ep", None),
        P(),
        P(None, "tp"),
        P("tp", None),
        P("tp", None),
        P("tp"),
        P("tp", None, None),
        P("tp", None, None),
        P("tp", None, None),
        P("tp", None, None),
        P("tp"),
        P("ep", "tp", None),
        P("ep", "tp", None),
        P("tp", None),
        P(),
        P(),
        P("ep", None),
        P(None, ("ep", "tp")),
        P(None, ("ep", "tp")),
        P("ep", "tp"),
    )
    out_specs = (P("ep", "tp"), P("ep", "tp", None), P("ep", "tp", None))
    return jax.shard_map(shards, mesh=mesh, in_specs=in_specs, out_specs=out_specs, check_vma=False)
```

profile of v0, /device:TPU:0, one launch (start us, length us, event | category | flops | bytes accessed | tf_op | source)
XLA Modules:
  0.0 71.3 jit_solution(13652618909060821899)
XLA Ops:
  0.6 0.0 copy-start
  0.7 0.8 %constant_dynamic-slice_fusion = s32[4,2]{0,1:T(2,128)S(1)} fusion(s32[32,2]{0,1:T(2,128)} %param.35, s32[]{:T(128)S(6)} %select_n.14), kind=kLoop, calls=%fused_computation.78 | loop fusion | bytes 68 | tf_op jit(solution)/shard_map/dynamic_slice | solution.py:124
  1.5 0.1 copy.71
  1.6 0.1 eq.56
  1.7 0.1 fusion.42
  1.7 0.7 exp.10
  2.4 0.9 %fusion.19 = f32[4]{0:T(128)S(1)} fusion(bf16[4,2048]{1,0:T(4,128)(2,1)} %param.20), kind=kLoop, calls=%fused_computation.32 | loop fusion | flops 24572 | bytes 16400 | tf_op jit(solution)/shard_map/reduce_sum | solution.py:16
  3.3 0.7 convert_element_type.68
  4.0 1.5 %convolution_convert_fusion.2 = bf16[4,256]{1,0:T(4,128)(2,1)S(1)} fusion(bf16[2048,256]{1,0:T(8,128)(2,1)} %param.22, bf16[4,2048]{1,0:T(4,128)(2,1)} %param.20, f32[2048]{0:T(1024)S(1)} %convert_element_type.68, f32[4]{0:T(128)S(1)} %add_rsqrt_fusion.1), kind=kOutput, calls=%fused_computation.13 | convolution fusion | flops 4228096 | bytes 1075216 | tf_op jit(solution)/shard_map/dot_general | solution.py:101
  5.5 0.1 reshape.72
  5.6 0.8 %cosine_multiply_fusion = (f32[16,64]{1,0:T(8,128)S(1)}, f32[16,64]{1,0:T(8,128)S(1)}, f32[16,64]{1,0:T(8,128)S(1)}, f32[16,64]{1,0:T(8,128)S(1)}) fusion(f32[16,64]{1,0:T(8,128)} %param.24, f32[16,64]{1,0:T(8,128)} %param.23, f32[16]{0:T(128)S(1)} %exp.10), kind=kLoop, calls=%fused_computation.51 | loop fusion | flops 17408 | bytes 24640 | tf_op jit(solution)/shard_map/mul | solution.py:26
  6.4 1.2 %fusion.2 = f32[4,16,64]{2,0,1:T(4,128)S(1)} fusion(f32[16,64,16]{1,2,0:T(8,128)} %param.26, f32[16,64,16]{1,2,0:T(8,128)} %param.27, f32[16,64]{1,0:T(8,128)S(1)} %get-tuple-element.21, f32[16,64]{1,0:T(8,128)S(1)} %get-tuple-element.20, f32[4,16,64]{2,1,0:T(8,128)} %param.32, f32[4,16,64]{2,1,0:T(8,128)} %param.31, f32[16,64]{1,0:T(8,128)S(1)} %get-tuple-element.22, ...), kind=kOutput, calls=%fused_computation.6 | convolution fusion | flops 851968 | bytes 198656 | tf_op jit(solution)/shard_map/sgp,gnp->sgn/dot_general | solution.py:57
  7.6 1.2 %fusion.3 = f32[4,16,64]{2,0,1:T(4,128)S(1)} fusion(f32[16,64,16]{1,2,0:T(8,128)} %param.27, f32[16,64,16]{1,2,0:T(8,128)} %param.26, f32[16,64]{1,0:T(8,128)S(1)} %get-tuple-element.21, f32[16,64]{1,0:T(8,128)S(1)} %get-tuple-element.20, f32[4,16,64]{2,1,0:T(8,128)} %param.32, f32[4,16,64]{2,1,0:T(8,128)} %param.31, f32[16,64]{1,0:T(8,128)S(1)} %get-tuple-element.22, ...), kind=kOutput, calls=%fused_computation.8 | convolution fusion | flops 851968 | bytes 198656 | tf_op jit(solution)/shard_map/sgp,gnp->sgn/dot_general | solution.py:56
  8.8 0.1 fusion.45
  8.9 0.1 fusion.43
  9.0 0.7 convert_element_type.80
  9.7 1.2 %fusion.60 = f32[16,4,16]{2,1,0:T(4,128)S(1)} fusion(f32[4,16,64]{2,0,1:T(4,128)S(1)} %fusion.3, f32[16,16,64]{2,1,0:T(8,128)} %param.28), kind=kOutput, calls=%fused_computation.84 | convolution fusion | flops 786432 | bytes 86016 | tf_op jit(solution)/shard_map/sgn,gpn->sgp/dot_general | solution.py:60
  10.9 1.2 %fusion.1 = f32[4,16,16]{2,0,1:T(4,128)S(1)} fusion(f32[16,4,16]{2,1,0:T(4,128)S(1)} %fusion.60, f32[4,16,64]{2,0,1:T(4,128)S(1)} %fusion.2, f32[16,16,64]{2,1,0:T(8,128)} %param.29), kind=kOutput, calls=%fused_computation.4 | convolution fusion | flops 787456 | bytes 90112 | tf_op jit(solution)/shard_map/sgn,gpn->sgp/dot_general | solution.py:60
  12.1 0.1 reshape.73
  12.2 0.0 copy-done
  12.2 0.9 %fusion.46 = f32[4,2048]{1,0:T(4,128)S(1)} fusion(bf16[256,2048]{1,0:T(8,128)(2,1)S(1)} %copy-done, f32[4,256]{1,0:T(4,128)S(1)} %reshape.73, bf16[4,256]{1,0:T(4,128)(2,1)S(1)} %convolution_convert_fusion.2, f32[256]{0:T(256)} %param.30), kind=kOutput, calls=%fused_computation.69 | convolution fusion | flops 4206592 | bytes 1088512 | tf_op jit(solution)/shard_map/dot_general | solution.py:117
  13.2 12.9 %psum.7 = f32[4,2048]{1,0:T(4,128)S(1)} all-reduce(f32[4,2048]{1,0:T(4,128)S(1)} %fusion.46), channel_id=1, replica_groups=mesh['ep'=8,'tp'=4] {'tp'}, use_global_device_ids=true, to_apply=%region_1.0 | all-reduce | flops 8192 | bytes 65536 | tf_op jit(solution)/shard_map/psum | solution.py:117
  26.1 0.9 %fusion.16 = (f32[4]{0:T(128)S(1)}, bf16[4,2048]{1,0:T(4,128)(2,1)S(1)}) fusion(f32[4,2048]{1,0:T(4,128)S(1)} %psum.7, bf16[4,2048]{1,0:T(4,128)(2,1)} %param.20), kind=kLoop, calls=%fused_computation.29 | loop fusion | flops 49148 | bytes 65552 | tf_op jit(solution)/shard_map/reduce_sum | solution.py:16
  26.9 0.8 %select_reduce_fusion.1 = (f32[4,8,2]{1,0,2:T(4,128)S(1)}, bf16[4,8,2]{1,0,2:T(4,128)(2,1)S(1)}) fusion(f32[4,2]{0,1:T(2,128)} %param.36, s32[4,2,8]{2,0,1:T(4,128)S(1)} %copy.73, pred[4,2,8]{2,0,1:T(4,128)(4,1)S(1)} %copy.74), kind=kLoop, calls=%fused_computation.45 | loop fusion | flops 640 | bytes 736 | tf_op jit(solution)/shard_map/reduce_sum | solution.py:74
  27.7 0.2 convolution_convert_fusion
  27.9 0.1 copy.75
  28.0 12.5 %all_to_all.10 = bf16[8,2,2048]{2,1,0:T(2,128)(2,1)S(1)} all-to-all(bf16[8,2,2048]{2,1,0:T(2,128)(2,1)S(1)} %copy.75), channel_id=1, replica_groups=mesh['ep'=8,'tp'=4] {'ep'}, dimensions={0} | all-to-all | bytes 131072 | tf_op jit(solution)/shard_map/all_to_all | solution.py:130
  40.5 4.6 %fusion.61 = f32[16,2048]{1,0:T(8,128)S(1)} fusion(bf16[16,2048]{1,0:T(8,128)(2,1)S(1)} %reshape.74, bf16[2048,2048]{1,0:T(8,128)(2,1)} %param.37), kind=kOutput, calls=%fused_computation.85 | convolution fusion | flops 134217728 | bytes 8585216 | tf_op jit(solution)/shard_map/dot_general | solution.py:134
  45.1 4.6 %fusion = bf16[16,2048]{1,0:T(8,128)(2,1)S(1)} fusion(bf16[16,2048]{1,0:T(8,128)(2,1)S(1)} %reshape.74, bf16[2048,2048]{1,0:T(8,128)(2,1)} %param.38, f32[16,2048]{1,0:T(8,128)S(1)} %fusion.61), kind=kOutput, calls=%fused_computation.2 | convolution fusion | flops 134414336 | bytes 8650752 | tf_op jit(solution)/shard_map/dot_general | solution.py:135
  49.7 5.8 %all_gather.3 = bf16[16,8192]{1,0:T(8,128)(2,1)S(1)} all-gather(bf16[16,2048]{1,0:T(8,128)(2,1)S(1)} %fusion), channel_id=1, replica_groups=mesh['ep'=8,'tp'=4] {'tp'}, dimensions={1}, use_global_device_ids=true | all-gather | bytes 327680 | tf_op jit(solution)/shard_map/all_gather | solution.py:139
  55.5 4.6 %convolution_convert_fusion.1 = bf16[16,512]{1,0:T(8,128)(2,1)S(1)} fusion(bf16[16,8192]{1,0:T(8,128)(2,1)S(1)} %all_gather.3, bf16[8192,512]{1,0:T(8,128)(2,1)} %param.39), kind=kOutput, calls=%fused_computation.9 | convolution fusion | flops 134225920 | bytes 8667136 | tf_op jit(solution)/shard_map/dot_general | solution.py:138
  60.0 0.6 reshape.75
  60.7 3.3 %all-to-all-start.1 = ((bf16[8,2,512]{2,1,0:T(2,128)(2,1)}), bf16[8,2,512]{2,1,0:T(2,128)(2,1)S(1)}, u32[]{:S(2)}, u32[]{:S(2)}) async-start(bf16[8,2,512]{2,1,0:T(2,128)(2,1)} %reshape.75), calls=%async_computation.1 | async-start | bytes 32768 | tf_op jit(solution)/shard_map/all_to_all | solution.py:144
  64.0 0.6 copy.77
  64.6 0.6 copy.78
  65.2 5.3 %all-to-all-done.1 = bf16[8,2,512]{2,1,0:T(2,128)(2,1)S(1)} async-done(((bf16[8,2,512]{2,1,0:T(2,128)(2,1)}), bf16[8,2,512]{2,1,0:T(2,128)(2,1)S(1)}, u32[]{:S(2)}, u32[]{:S(2)}) %all-to-all-start.1) | async-done | bytes 16416 | tf_op jit(solution)/shard_map/all_to_all | solution.py:144
  70.5 0.8 %fusion.5 = bf16[4,512]{1,0:T(4,128)(2,1)} fusion(bf16[8,2,512]{2,1,0:T(2,128)(2,1)S(1)} %all-to-all-done.1, f32[4,8,2]{1,0,2:T(4,128)S(1)} %get-tuple-element.15, bf16[4,2048]{1,0:T(4,128)(2,1)S(1)} %get-tuple-element.18, s32[]{:T(128)S(6)} %select_n.13), kind=kOutput, calls=%fused_computation.12 | convolution fusion | flops 399360 | bytes 24836 | tf_op jit(solution)/shard_map/xcs,xcd->sd/dot_general | solution.py:149
  (7 shorter events, 0.1 us)
Async XLA Ops:
  0.6 11.6 %copy-start = (bf16[256,2048]{1,0:T(8,128)(2,1)S(1)}, bf16[256,2048]{1,0:T(8,128)(2,1)}, u32[]{:S(2)}) copy-start(bf16[256,2048]{1,0:T(8,128)(2,1)} %param.33) | copy-start | bytes 3145732
  60.7 9.9 %all-to-all-start.1 = ((bf16[8,2,512]{2,1,0:T(2,128)(2,1)}), bf16[8,2,512]{2,1,0:T(2,128)(2,1)S(1)}, u32[]{:S(2)}, u32[]{:S(2)}) async-start(bf16[8,2,512]{2,1,0:T(2,128)(2,1)} %reshape.75), calls=%async_computation.1 | async-start | bytes 32768 | tf_op jit(solution)/shard_map/all_to_all | solution.py:144
where the time goes:
time: 72.1 us; the launch traced here: 71.3 us
  blocking collectives  31.2 us (43%)
  matrix products  22 us (31%)
  waiting for transfers between devices  5.28 us (7%)
  other arithmetic  4.97 us (7%)
  local copies, waits for them, and re-layouts  3.84 us (5%)
  starting transfers between devices  3.33 us (5%)
  between operations  0.73 us (1%)
    psum x1, blocking collectives, shards(): lax.psum(jnp.dot(activated, out_weight, preferred_element_type=jnp.float3...  12.9 us
    all_to_all x1, blocking collectives, shards(): lax.all_to_all(jnp.repeat(outgoing, group_span, axis=0), 'ep', split_axis...  12.5 us
    all_gather x1, blocking collectives, shards(): lax.all_gather(hidden, 'tp', axis=1, tiled=True)  5.77 us
    all_to_all x1, waiting for transfers between devices, shards(): lax.all_to_all(rounded, 'ep', split_axis=0, concat_axis=0, tiled=True)  5.28 us
    dot_general x1, matrix products, shards(): up_pre = jnp.dot(slot_rows, up_weight, preferred_element_type=jnp.float32)  4.58 us
    dot_general x1, matrix products, shards(): jnp.dot(slot_rows, gate_weight, preferred_element_type=jnp.float32)  4.58 us
    dot_general x1, matrix products, shards(): jnp.dot(lax.all_gather(hidden, 'tp', axis=1, tiled=True), down_weight, pr...  4.56 us
    all_to_all x1, starting transfers between devices, shards(): lax.all_to_all(rounded, 'ep', split_axis=0, concat_axis=0, tiled=True)  3.33 us
  transfers between devices with their start and end apart: 1, of which 1 were waited for; matrix products, arithmetic and copies ran while one was open for 2% of the time, Pallas kernels for 0%

commit v1 on v0

v1 whole, which is shorter than its diff:
```python
import jax
import jax.numpy as jnp
from jax import lax
from jax.experimental import pallas as pl
from jax.experimental.pallas import tpu as pltpu
from jax.sharding import PartitionSpec as P

EXPERTS = 8
EPSILON = 1e-06
F32 = jnp.float32
BF16 = jnp.bfloat16
MIB = 1 << 20
PIECES = 4


def dot(a, b, contract=((1,), (0,))):
    return lax.dot_general(a, b, (contract, ((), ())), preferred_element_type=F32)


def split_high_low(values):
    high = values.astype(BF16)
    return high, (values - high.astype(F32)).astype(BF16)


def rms_norm(floats, gain):
    scale = lax.rsqrt(jnp.mean(floats * floats, axis=-1, keepdims=True) + EPSILON)
    return (floats * scale * gain.astype(F32)).astype(BF16)


def repeat_rows(values, count):
    rows = [
        jnp.broadcast_to(values[s : s + 1], (count, values.shape[1]))
        for s in range(values.shape[0])
    ]
    return jnp.concatenate(rows, axis=0)


def slot_tables(base, ids, weights, count, slots):
    total = ids.shape[1]
    pick = (total, count)
    own = lax.broadcasted_iota(jnp.int32, pick, 0) == base + lax.broadcasted_iota(
        jnp.int32, pick, 1
    )
    own_ids = dot(ids.astype(F32).astype(BF16), own.astype(F32).astype(BF16))
    shape = (EXPERTS * slots, count)
    row = lax.broadcasted_iota(jnp.int32, shape, 0)
    expert = (row // slots).astype(F32)
    place = (row % slots).astype(F32)
    hits = jnp.zeros(shape, F32)
    scaled = jnp.zeros(shape, F32)
    for k in range(ids.shape[0]):
        same = jnp.broadcast_to(own_ids[k : k + 1], shape) == expert
        hits = hits + jnp.where(same, 1.0, 0.0)
        scaled = scaled + jnp.where(same, jnp.broadcast_to(weights[k : k + 1], shape), 0.0)
    earlier = (count, count)
    upper = lax.broadcasted_iota(jnp.int32, earlier, 0) < lax.broadcasted_iota(
        jnp.int32, earlier, 1
    )
    before = dot(hits.astype(BF16), upper.astype(F32).astype(BF16))
    placed = before == place
    return jnp.where(placed, hits, 0.0), jnp.where(placed, scaled, 0.0)


def as_row(values):
    rows = values.astype(F32)
    return jnp.concatenate([rows[j : j + 1] for j in range(rows.shape[0])], axis=1)


MIXER_INPUTS = 17


def mixer_kernel(base, *refs):
    sources, refs = refs[:MIXER_INPUTS], refs[MIXER_INPUTS:]
    partial, new_real, new_imag, kept_tokens, kept_gain, select, table = refs[:7]
    buffers, sems = refs[7:-1], refs[-1]
    copies = [
        pltpu.make_async_copy(source, buffer, sems.at[i])
        for i, (source, buffer) in enumerate(zip(sources, buffers))
    ]
    for copy in copies:
        copy.start()
    (
        tokens,
        norm_gain,
        in_weight,
        decay_rate,
        frequency,
        log_step,
        input_real,
        input_imag,
        output_real,
        output_imag,
        skip_gain,
        state_real,
        state_imag,
        ffn_gain,
        ids,
        weights,
        out_weight,
    ) = buffers
    for copy in copies[:-1]:
        copy.wait()
    kept_tokens[...] = tokens[...]
    kept_gain[...] = as_row(ffn_gain[...])
    selected, scaled = slot_tables(
        base[0], ids[...], weights[...], tokens.shape[0], select.shape[0] // EXPERTS
    )
    select[...] = selected
    table[...] = scaled
    count = tokens.shape[0]
    groups, states = decay_rate.shape
    channels = in_weight.shape[1]
    width = channels // groups
    normed = rms_norm(tokens[...].astype(F32), as_row(norm_gain[...]))
    projected = dot(normed, in_weight[...]).astype(BF16).astype(F32)
    shape = (count * groups, channels)
    row_group = lax.broadcasted_iota(jnp.int32, shape, 0) % groups
    own_group = row_group == lax.broadcasted_iota(jnp.int32, shape, 1) // width
    spread = jnp.where(own_group, repeat_rows(projected, groups), 0.0).astype(BF16)
    inputs = jnp.concatenate([input_real[...], input_imag[...]], axis=1)
    inputs_high, inputs_low = split_high_low(inputs)
    driven = dot(spread, inputs_high) + dot(spread, inputs_low)
    driven_real, driven_imag = driven[:, :states], driven[:, states:]

    square = (groups, groups)
    diagonal = lax.broadcasted_iota(jnp.int32, square, 0) == lax.broadcasted_iota(
        jnp.int32, square, 1
    )
    step_size = jnp.exp(
        jnp.sum(
            jnp.where(diagonal, jnp.broadcast_to(log_step[...], square), 0.0),
            axis=1,
            keepdims=True,
        )
    )
    lam_real = -decay_rate[...]
    lam_imag = frequency[...]
    magnitude = jnp.exp(lam_real * step_size)
    turned = lam_imag * step_size
    bar_real = magnitude * jnp.cos(turned)
    bar_imag = magnitude * jnp.sin(turned)
    denom = lam_real * lam_real + lam_imag * lam_imag
    minus_one = bar_real - 1.0
    factor_real = (minus_one * lam_real + bar_imag * lam_imag) / denom
    factor_imag = (bar_imag * lam_real - minus_one * lam_imag) / denom
    bar_real, bar_imag, factor_real, factor_imag = (
        jnp.concatenate([v] * count, axis=0)
        for v in (bar_real, bar_imag, factor_real, factor_imag)
    )
    old_real, old_imag = state_real[...], state_imag[...]
    fresh_real = (
        bar_real * old_real
        - bar_imag * old_imag
        + factor_real * driven_real
        - factor_imag * driven_imag
    )
    fresh_imag = (
        bar_real * old_imag
        + bar_imag * old_real
        + factor_real * driven_imag
        + factor_imag * driven_real
    )
    new_real[...] = fresh_real
    new_imag[...] = fresh_imag

    fresh_high, fresh_low = split_high_low(jnp.concatenate([fresh_real, fresh_imag], axis=1))
    out_high, out_low = split_high_low(
        jnp.concatenate([output_real[...], -output_imag[...]], axis=1)
    )
    across = ((1,), (1,))
    read = (
        dot(fresh_high, out_high, across)
        + dot(fresh_low, out_high, across)
        + dot(fresh_high, out_low, across)
    )
    read = jnp.where(own_group, read, 0.0)
    read = jnp.concatenate(
        [
            jnp.sum(read[s * groups : (s + 1) * groups], axis=0, keepdims=True)
            for s in range(count)
        ],
        axis=0,
    )
    activated = jax.nn.gelu(read + skip_gain[...] * projected).astype(BF16)
    copies[-1].wait()
    partial[...] = dot(activated, out_weight[...])


def prefetch_kernel(order, gate, up, gate_copy, up_copy, sems):
    del order
    pairs = []
    for source, target in ((gate, gate_copy), (up, up_copy)):
        part = source.shape[0] // PIECES
        for j in range(PIECES):
            rows = pl.ds(j * part, part)
            pairs.append((source.at[rows], target.at[rows]))
    copies = [pltpu.make_async_copy(a, b, sems.at[i]) for i, (a, b) in enumerate(pairs)]
    for copy in copies:
        copy.start()
    for copy in copies:
        copy.wait()


def dispatch_kernel(*refs):
    shares, (tokens, gain, select, _, _, outgoing, hidden) = refs[:-7], refs[-7:]
    slots = outgoing.shape[1]
    delta = shares[0][...]
    for share in shares[1:]:
        delta = delta + share[...]
    hidden_state = (tokens[...].astype(F32) + delta).astype(BF16)
    hidden[...] = hidden_state
    normed = rms_norm(hidden_state.astype(F32), gain[...])
    sent = dot(select[...].astype(BF16), normed).astype(BF16)
    for x in range(EXPERTS):
        outgoing[x] = sent[x * slots : (x + 1) * slots]


def hidden_kernel(received, gate, up, hidden):
    rows = jnp.concatenate([received[x] for x in range(received.shape[0])], axis=0)
    gate_pre = dot(rows, gate[...])
    up_pre = dot(rows, up[...])
    hidden[...] = (jax.nn.silu(gate_pre) * up_pre).astype(BF16)


def down_kernel(hidden, down, out):
    units = hidden.shape[2]
    total = dot(hidden[0], down[:units])
    for j in range(1, hidden.shape[0]):
        total = total + dot(hidden[j], down[j * units : (j + 1) * units])
    rounded = total.astype(BF16)
    slots = out.shape[1]
    for x in range(out.shape[0]):
        out[x] = rounded[x * slots : (x + 1) * slots]


def combine_kernel(start, returned, table, hidden, mixed):
    quarter = mixed.shape[1]
    rows = jnp.concatenate([returned[x] for x in range(returned.shape[0])], axis=0)
    routed = lax.dot_general(
        table[...],
        rows.astype(F32),
        (((0,), (0,)), ((), ())),
        precision=lax.Precision.HIGHEST,
        preferred_element_type=F32,
    )
    first = pl.multiple_of(start[0], 128)
    residual = hidden[:, pl.ds(first, quarter)].astype(F32)
    mixed[...] = (residual + routed).astype(BF16)


def call(kernel, out, args, limit, scalars=0):
    specs = [pl.BlockSpec(memory_space=pltpu.SMEM)] * scalars
    specs = specs + [pl.BlockSpec(memory_space=pltpu.VMEM)] * (len(args) - scalars)
    return pl.pallas_call(
        kernel,
        out_shape=out,
        in_specs=specs,
        compiler_params=pltpu.CompilerParams(vmem_limit_bytes=limit * MIB),
    )(*args)


def shards(
    tokens,
    norm_gain,
    in_weight,
    decay_rate,
    frequency,
    log_step,
    input_real,
    input_imag,
    output_real,
    output_imag,
    skip_gain,
    state_real,
    state_imag,
    out_weight,
    ffn_gain,
    expert_ids,
    route_weights,
    gate_weight,
    up_weight,
    down_weight,
):
    count, width = tokens.shape
    groups, states = decay_rate.shape
    channels = in_weight.shape[1]
    quarter = down_weight.shape[1]
    flat_state = (count * groups, states)
    struct = jax.ShapeDtypeStruct
    slots = count // 2
    base = jnp.reshape(lax.axis_index("ep") * count, (1,)).astype(jnp.int32)
    start = jnp.reshape(lax.axis_index("tp") * quarter, (1,)).astype(jnp.int32)
    sources = (
        tokens,
        norm_gain.reshape(-1, 128),
        in_weight,
        decay_rate,
        frequency,
        log_step[None],
        jnp.swapaxes(input_real, 1, 2).reshape(channels, states),
        jnp.swapaxes(input_imag, 1, 2).reshape(channels, states),
        output_real.reshape(channels, states),
        output_imag.reshape(channels, states),
        skip_gain[None],
        state_real.reshape(flat_state),
        state_imag.reshape(flat_state),
        ffn_gain.reshape(-1, 128),
        expert_ids.T,
        route_weights.T,
        out_weight,
    )
    hbm = pl.BlockSpec(memory_space=pltpu.HBM)
    vmem = pl.BlockSpec(memory_space=pltpu.VMEM)
    smem = pl.BlockSpec(memory_space=pltpu.SMEM)
    table_shape = struct((EXPERTS * slots, count), F32)
    partial, new_real, new_imag, kept_tokens, kept_gain, select, table = pl.pallas_call(
        mixer_kernel,
        out_shape=(
            struct((count, width), F32),
            struct(flat_state, F32),
            struct(flat_state, F32),
            struct((count, width), BF16),
            struct((1, width), F32),
            table_shape,
            table_shape,
        ),
        in_specs=[smem] + [hbm] * len(sources),
        scratch_shapes=[pltpu.VMEM(v.shape, v.dtype) for v in sources]
        + [pltpu.SemaphoreType.DMA((len(sources),))],
        compiler_params=pltpu.CompilerParams(vmem_limit_bytes=10 * MIB),
    )(base, *[pltpu.with_memory_space_constraint(v, pltpu.HBM) for v in sources])
    ways = lax.axis_size("tp")
    shares = [partial] + [
        lax.ppermute(partial, "tp", [(i, (i + k) % ways) for i in range(ways)])
        for k in range(1, ways)
    ]
    gate_here, up_here = pl.pallas_call(
        prefetch_kernel,
        out_shape=(
            struct(gate_weight.shape, BF16),
            struct(up_weight.shape, BF16),
        ),
        in_specs=[vmem, hbm, hbm],
        out_specs=(vmem, vmem),
        scratch_shapes=[pltpu.SemaphoreType.DMA((2 * PIECES,))],
        compiler_params=pltpu.CompilerParams(vmem_limit_bytes=1 * MIB),
    )(
        select,
        pltpu.with_memory_space_constraint(gate_weight, pltpu.HBM),
        pltpu.with_memory_space_constraint(up_weight, pltpu.HBM),
    )
    outgoing, hidden_state = call(
        dispatch_kernel,
        (struct((EXPERTS, slots, width), BF16), struct((count, width), BF16)),
        (*shares, kept_tokens, kept_gain, select, gate_here, up_here),
        4,
    )
    span = lax.axis_size("ep") // EXPERTS
    if span > 1:
        outgoing = jnp.repeat(outgoing, span, axis=0)
    received = lax.all_to_all(outgoing, "ep", split_axis=0, concat_axis=0, tiled=True)
    peers = received.shape[0]
    hidden = call(
        hidden_kernel,
        struct((peers * slots, gate_weight.shape[1]), BF16),
        (received, gate_here, up_here),
        4,
    )
    out = call(
        down_kernel,
        struct((peers, slots, quarter), BF16),
        (lax.all_gather(hidden, "tp"), down_weight),
        6,
    )
    returned = lax.all_to_all(out, "ep", split_axis=0, concat_axis=0, tiled=True)
    if span > 1:
        returned = returned.astype(F32).reshape(EXPERTS, span, slots, quarter).sum(axis=1)
    mixed = call(
        combine_kernel,
        struct((count, quarter), BF16),
        (start, returned, table, hidden_state),
        2,
        1,
    )
    shape = state_real.shape
    return (mixed, new_real.reshape(shape), new_imag.reshape(shape))

def solution(mesh):
    in_specs = (
        P("ep", None),
        P(),
        P(None, "tp"),
        P("tp", None),
        P("tp", None),
        P("tp"),
        P("tp", None, None),
        P("tp", None, None),
        P("tp", None, None),
        P("tp", None, None),
        P("tp"),
        P("ep", "tp", None),
        P("ep", "tp", None),
        P("tp", None),
        P(),
        P(),
        P("ep", None),
        P(None, ("ep", "tp")),
        P(None, ("ep", "tp")),
        P("ep", "tp"),
    )
    out_specs = (P("ep", "tp"), P("ep", "tp", None), P("ep", "tp", None))
    return jax.shard_map(shards, mesh=mesh, in_specs=in_specs, out_specs=out_specs, check_vma=False)
```

time: 72.1 us -> 47.3 us (0.66)
  matrix products: 22 us -> 0 us
  Pallas kernels: 0 us -> 14.3 us
  blocking collectives: 31.2 us -> 18.9 us
  other arithmetic: 4.97 us -> 0.01 us
  local copies, waits for them, and re-layouts: 3.84 us -> 0.01 us
  starting transfers between devices: 3.33 us -> 6.6 us
  waiting for transfers between devices: 5.28 us -> 6.52 us
    dot_general x11 -> x0, matrix products: 22 us -> none  [the longest x1 4.58 us: shards(): up_pre = jnp.dot(slot_rows, up_weight, preferred_element_type=jnp.float32)]
    pallas_call x0 -> x6, Pallas kernels: none -> 14.3 us  [the longest x1 5.92 us: shards(): pl.pallas_call(prefetch_kernel, out_shape=(struct(gate_weight.shape, BF16...]
    psum x1 -> x0, blocking collectives: 12.9 us -> none  [shards(): lax.psum(jnp.dot(activated, out_weight, preferred_element_type=jnp.float3...]
    ppermute x0 -> x3, starting transfers between devices: none -> 3.28 us  [shards(): lax.ppermute(partial, 'tp', [(i, (i + k) % ways) for i in range(ways)])]
    reduce_sum x3 -> x0, other arithmetic: 2.47 us -> none  [the longest x2 1.7 us: rms_scale(): jnp.mean(floats * floats, axis=-1, keepdims=True) + EPSILON]
    convert_element_type x3 -> x0, other arithmetic: 1.46 us -> none  [the longest x2 1.38 us: rms_scale(): gain.astype(jnp.float32)]
    unnamed x4, local copies, waits for them, and re-layouts: 1.24 us -> 0.01 us
    all_to_all x1, waiting for transfers between devices: 5.28 us -> 6.51 us  [shards(): lax.all_to_all(out, 'ep', split_axis=0, concat_axis=0, tiled=True)]
  transfers between devices with their start and end apart: 1 -> 4, of which waited for: 1 -> 1; matrix products, arithmetic and copies ran while one was open for 2% -> 0% of each run, Pallas kernels for 0% -> 13%
where the time goes in v1:
time: 47.3 us; the launch traced here: 47 us
  blocking collectives  18.9 us (40%)
  Pallas kernels  14.3 us (30%)
  starting transfers between devices  6.6 us (14%)
  waiting for transfers between devices  6.52 us (14%)
  between operations  0.72 us (2%)
    all_to_all x1, blocking collectives, shards(): lax.all_to_all(outgoing, 'ep', split_axis=0, concat_axis=0, tiled=True)  13.1 us
    all_to_all x1, waiting for transfers between devices, shards(): lax.all_to_all(out, 'ep', split_axis=0, concat_axis=0, tiled=True)  6.51 us
    pallas_call x1, Pallas kernels, shards(): pl.pallas_call(prefetch_kernel, out_shape=(struct(gate_weight.shape, BF16...  5.92 us
    all_gather x1, blocking collectives, shards(): lax.all_gather(hidden, 'tp')  5.77 us
    pallas_call x4, Pallas kernels, call(): pl.pallas_call(kernel, out_shape=out, in_specs=specs, compiler_params=plt...  5.14 us
    all_to_all x1, starting transfers between devices, shards(): lax.all_to_all(out, 'ep', split_axis=0, concat_axis=0, tiled=True)  3.32 us
    ppermute x3, starting transfers between devices, shards(): lax.ppermute(partial, 'tp', [(i, (i + k) % ways) for i in range(ways)])  3.28 us
    pallas_call x1, Pallas kernels, shards(): pl.pallas_call(mixer_kernel, out_shape=(struct((count, width), F32), stru...  3.24 us
  transfers between devices with their start and end apart: 4, of which 1 were waited for; matrix products, arithmetic and copies ran while one was open for 0% of the time, Pallas kernels for 13%

profile of v1, /device:TPU:0, one launch (start us, length us, event | category | flops | bytes accessed | tf_op | source)
XLA Modules:
  0.0 47.0 jit_solution(496782708532212044)
XLA Ops:
  0.6 3.2 %shard_map.211 = (f32[4,2048]{1,0:T(4,128)S(1)}, f32[64,64]{1,0:T(8,128)}, f32[64,64]{1,0:T(8,128)}, bf16[4,2048]{1,0:T(4,128)(2,1)S(1)}, f32[1,2048]{1,0:T(1,12...) custom-call(s32[1]{0:T(128)} %bitcast.1.base, bf16[4,2048]{1,0:T(4,128)(2,1)} %refs_0_.1, bf16[16,128]{1,0:T(8,128)(2,1)} %bitcast.30, ...), custom_call_target="tpu_custom_call" | custom-call | tf_op jit(solution)/shard_map/pallas_call | solution.py:316
  3.9 2.5 %collective-permute-start.2 = (f32[4,2048]{1,0:T(4,128)S(1)}, f32[4,2048]{1,0:T(4,128)S(1)}, u32[]{:S(2)}, u32[]{:S(2)}) collective-permute-start(f32[4,2048]{1,0:T(4,128)S(1)} %get-tuple-element.14.refs_0_), channel_id=1, source_target_pairs={{0,3},{1,0},{2,1},{3,2},{4,7},{5,4},{6,5},{7,6},{8,11},{9,8},{10,9... | collective-permute-start | bytes 98312 | tf_op jit(solution)/shard_map/ppermute | solution.py:334
  6.4 0.6 %collective-permute-start.1 = (f32[4,2048]{1,0:T(4,128)S(1)}, f32[4,2048]{1,0:T(4,128)S(1)}, u32[]{:S(2)}, u32[]{:S(2)}) collective-permute-start(f32[4,2048]{1,0:T(4,128)S(1)} %get-tuple-element.14.refs_0_), channel_id=1, source_target_pairs={{0,2},{1,3},{2,0},{3,1},{4,6},{5,7},{6,4},{7,5},{8,10},{9,11},{10,... | collective-permute-start | bytes 98312 | tf_op jit(solution)/shard_map/ppermute | solution.py:334
  7.0 0.2 collective-permute-start
  7.2 5.9 %shard_map.212 = (bf16[2048,2048]{1,0:T(8,128)(2,1)S(1)}, bf16[2048,2048]{1,0:T(8,128)(2,1)S(1)}) custom-call(f32[16,4]{1,0:T(8,128)S(1)} %get-tuple-element.17.order.refs_6_, bf16[2048,2048]{1,0:T(8,128)(2,1)} %gate.1, bf16[2048,2048]{1,0:T(8,128)(2,1)} %up.1), custom_call_target="tpu_custom_call" | custom-call | tf_op jit(solution)/shard_map/pallas_call | solution.py:337
  13.1 0.0 collective-permute-done.2.refs_3_
  13.1 0.0 collective-permute-done.1.refs_2_
  13.1 0.0 collective-permute-done.refs_1_
  13.1 0.0 slice-start
  13.1 0.3 shard_map.213
  13.4 13.1 %all_to_all.10.received = bf16[8,2,2048]{2,1,0:T(2,128)(2,1)S(1)} all-to-all(bf16[8,2,2048]{2,1,0:T(2,128)(2,1)S(1)} %get-tuple-element.20), channel_id=1, replica_groups=mesh['ep'=8,'tp'=4] {'ep'}, dimensions={0} | all-to-all | bytes 131072 | tf_op jit(solution)/shard_map/all_to_all | solution.py:361
  26.5 0.0 slice-start.1
  26.5 2.3 %shard_map.214 = bf16[16,2048]{1,0:T(8,128)(2,1)S(1)} custom-call(bf16[8,2,2048]{2,1,0:T(2,128)(2,1)S(1)} %all_to_all.10.received, bf16[2048,2048]{1,0:T(8,128)(2,1)S(1)} %get-tuple-element.18.refs_7_.gate, bf16[2048,2048]{1,0:T(8,128)(2,1)S(1)} %get-tuple-element.19.refs_8_.up), custom_call_target="tpu_custom_call" | custom-call | tf_op jit(solution)/shard_map/pallas_call | solution.py:254
  28.8 5.8 %all-gather = bf16[64,2048]{1,0:T(8,128)(2,1)S(1)} all-gather(bf16[16,2048]{1,0:T(8,128)(2,1)S(1)} %shard_map.214), channel_id=2, replica_groups=mesh['ep'=8,'tp'=4] {'tp'}, dimensions={0}, use_global_device_ids=true | all-gather | bytes 327680 | tf_op jit(solution)/shard_map/all_gather | solution.py:372
  34.6 0.0 slice-done
  34.6 0.0 slice-done.1
  34.6 1.8 %shard_map.215 = bf16[8,2,512]{2,1,0:T(2,128)(2,1)} custom-call(bf16[4,16,2048]{2,1,0:T(8,128)(2,1)S(1)} %bitcast.23, bf16[8192,512]{1,0:T(8,128)(2,1)S(1)} %bitcast.22), custom_call_target="tpu_custom_call" | custom-call | tf_op jit(solution)/shard_map/pallas_call | solution.py:254
  36.4 3.3 %all-to-all-start.1 = ((bf16[8,2,512]{2,1,0:T(2,128)(2,1)}), bf16[8,2,512]{2,1,0:T(2,128)(2,1)S(1)}, u32[]{:S(2)}, u32[]{:S(2)}) async-start(bf16[8,2,512]{2,1,0:T(2,128)(2,1)} %shard_map.215), calls=%async_computation.1 | async-start | bytes 32768 | tf_op jit(solution)/shard_map/all_to_all | solution.py:375
  39.7 6.5 %all-to-all-done.1.returned = bf16[8,2,512]{2,1,0:T(2,128)(2,1)S(1)} async-done(((bf16[8,2,512]{2,1,0:T(2,128)(2,1)}), bf16[8,2,512]{2,1,0:T(2,128)(2,1)S(1)}, u32[]{:S(2)}, u32[]{:S(2)}) %all-to-all-start.1) | async-done | bytes 16416 | tf_op jit(solution)/shard_map/all_to_all | solution.py:375
  46.2 0.8 %shard_map.216 = bf16[4,512]{1,0:T(4,128)(2,1)} custom-call(s32[1]{0:T(128)} %bitcast.start, bf16[8,2,512]{2,1,0:T(2,128)(2,1)S(1)} %all-to-all-done.1.returned, f32[16,4]{1,0:T(8,128)S(1)} %get-tuple-element.21.table, bf16[4,2048]{1,0:T(4,128)(2,1)S(1)} %get-tuple-element.22.hidden), custom_call_target="tpu_custom_call" | custom-call | tf_op jit(solution)/shard_map/pallas_call | solution.py:254
  (1 shorter events, 0.0 us)
Async XLA Ops:
  3.9 9.2 %collective-permute-start.2 = (f32[4,2048]{1,0:T(4,128)S(1)}, f32[4,2048]{1,0:T(4,128)S(1)}, u32[]{:S(2)}, u32[]{:S(2)}) collective-permute-start(f32[4,2048]{1,0:T(4,128)S(1)} %get-tuple-element.14.refs_0_), channel_id=1, source_target_pairs={{0,3},{1,0},{2,1},{3,2},{4,7},{5,4},{6,5},{7,6},{8,11},{9,8},{10,9... | collective-permute-start | bytes 98312 | tf_op jit(solution)/shard_map/ppermute | solution.py:334
  6.4 6.7 %collective-permute-start.1 = (f32[4,2048]{1,0:T(4,128)S(1)}, f32[4,2048]{1,0:T(4,128)S(1)}, u32[]{:S(2)}, u32[]{:S(2)}) collective-permute-start(f32[4,2048]{1,0:T(4,128)S(1)} %get-tuple-element.14.refs_0_), channel_id=1, source_target_pairs={{0,2},{1,3},{2,0},{3,1},{4,6},{5,7},{6,4},{7,5},{8,10},{9,11},{10,... | collective-permute-start | bytes 98312 | tf_op jit(solution)/shard_map/ppermute | solution.py:334
  7.0 6.1 %collective-permute-start = (f32[4,2048]{1,0:T(4,128)S(1)}, f32[4,2048]{1,0:T(4,128)S(1)}, u32[]{:S(2)}, u32[]{:S(2)}) collective-permute-start(f32[4,2048]{1,0:T(4,128)S(1)} %get-tuple-element.14.refs_0_), channel_id=1, source_target_pairs={{0,1},{1,2},{2,3},{3,0},{4,5},{5,6},{6,7},{7,4},{8,9},{9,10},{10,1... | collective-permute-start | bytes 98312 | tf_op jit(solution)/shard_map/ppermute | solution.py:334
  13.1 21.4 %slice-start = ((s8[8388608]{0:T(1024)(128)(4,1)}), s8[4194304]{0:T(1024)(128)(4,1)S(1)}, s32[]{:S(2)}) async-start(s8[8388608]{0:T(1024)(128)(4,1)} %bitcast.21), calls=%async_computation.2 | async-start | bytes 8388608
  26.5 8.1 %slice-start.1 = ((s8[8388608]{0:T(1024)(128)(4,1)}), s8[4194304]{0:T(1024)(128)(4,1)S(1)}, s32[]{:S(2)}) async-start(s8[8388608]{0:T(1024)(128)(4,1)} %bitcast.21), calls=%async_computation.3 | async-start | bytes 8388608
  36.4 9.8 %all-to-all-start.1 = ((bf16[8,2,512]{2,1,0:T(2,128)(2,1)}), bf16[8,2,512]{2,1,0:T(2,128)(2,1)S(1)}, u32[]{:S(2)}, u32[]{:S(2)}) async-start(bf16[8,2,512]{2,1,0:T(2,128)(2,1)} %shard_map.215), calls=%async_computation.1 | async-start | bytes 32768 | tf_op jit(solution)/shard_map/all_to_all | solution.py:375

commit v2 on v1

--- a/solution.py
+++ b/solution.py
@@ -10,7 +10,6 @@
 F32 = jnp.float32
 BF16 = jnp.bfloat16
 MIB = 1 << 20
-PIECES = 4
 
 
 def dot(a, b, contract=((1,), (0,))):
@@ -186,27 +185,12 @@
     partial[...] = dot(activated, out_weight[...])
 
 
-def prefetch_kernel(order, gate, up, gate_copy, up_copy, sems):
-    del order
-    pairs = []
-    for source, target in ((gate, gate_copy), (up, up_copy)):
-        part = source.shape[0] // PIECES
-        for j in range(PIECES):
-            rows = pl.ds(j * part, part)
-            pairs.append((source.at[rows], target.at[rows]))
-    copies = [pltpu.make_async_copy(a, b, sems.at[i]) for i, (a, b) in enumerate(pairs)]
-    for copy in copies:
-        copy.start()
-    for copy in copies:
-        copy.wait()
-
-
-def dispatch_kernel(*refs):
-    shares, (tokens, gain, select, _, _, outgoing, hidden) = refs[:-7], refs[-7:]
+def dispatch_kernel(gathered, tokens, gain, select, gate, up, outgoing, hidden):
+    del gate, up
     slots = outgoing.shape[1]
-    delta = shares[0][...]
-    for share in shares[1:]:
-        delta = delta + share[...]
+    delta = gathered[0]
+    for j in range(1, gathered.shape[0]):
+        delta = delta + gathered[j]
     hidden_state = (tokens[...].astype(F32) + delta).astype(BF16)
     hidden[...] = hidden_state
     normed = rms_norm(hidden_state.astype(F32), gain[...])
@@ -329,31 +313,19 @@
         + [pltpu.SemaphoreType.DMA((len(sources),))],
         compiler_params=pltpu.CompilerParams(vmem_limit_bytes=10 * MIB),
     )(base, *[pltpu.with_memory_space_constraint(v, pltpu.HBM) for v in sources])
-    ways = lax.axis_size("tp")
-    shares = [partial] + [
-        lax.ppermute(partial, "tp", [(i, (i + k) % ways) for i in range(ways)])
-        for k in range(1, ways)
-    ]
-    gate_here, up_here = pl.pallas_call(
-        prefetch_kernel,
-        out_shape=(
-            struct(gate_weight.shape, BF16),
-            struct(up_weight.shape, BF16),
-        ),
-        in_specs=[vmem, hbm, hbm],
-        out_specs=(vmem, vmem),
-        scratch_shapes=[pltpu.SemaphoreType.DMA((2 * PIECES,))],
-        compiler_params=pltpu.CompilerParams(vmem_limit_bytes=1 * MIB),
+    gathered = lax.all_gather(partial, "tp")
+    outgoing, hidden_state = pl.pallas_call(
+        dispatch_kernel,
+        out_shape=(struct((EXPERTS, slots, width), BF16), struct((count, width), BF16)),
+        in_specs=[vmem] * 4 + [hbm] * 2,
+        compiler_params=pltpu.CompilerParams(vmem_limit_bytes=4 * MIB),
     )(
+        gathered,
+        kept_tokens,
+        kept_gain,
         select,
         pltpu.with_memory_space_constraint(gate_weight, pltpu.HBM),
         pltpu.with_memory_space_constraint(up_weight, pltpu.HBM),
-    )
-    outgoing, hidden_state = call(
-        dispatch_kernel,
-        (struct((EXPERTS, slots, width), BF16), struct((count, width), BF16)),
-        (*shares, kept_tokens, kept_gain, select, gate_here, up_here),
-        4,
     )
     span = lax.axis_size("ep") // EXPERTS
     if span > 1:
@@ -363,7 +335,7 @@
     hidden = call(
         hidden_kernel,
         struct((peers * slots, gate_weight.shape[1]), BF16),
-        (received, gate_here, up_here),
+        (received, gate_weight, up_weight),
         4,
     )
     out = call(

time: 47.3 us -> 44.7 us (0.945)
  blocking collectives: 18.9 us -> 25.4 us
  Pallas kernels: 14.3 us -> 8.52 us
  starting transfers between devices: 6.6 us -> 3.31 us
    all_gather x0 -> x1, blocking collectives: none -> 6.54 us  [shards(): gathered = lax.all_gather(partial, 'tp')]
    pallas_call x1, Pallas kernels: 5.92 us -> 0.25 us  [shards(): pl.pallas_call(dispatch_kernel, out_shape=(struct((EXPERTS, slots, width)...]
    ppermute x3 -> x0, starting transfers between devices: 3.28 us -> none  [shards(): lax.ppermute(partial, 'tp', [(i, (i + k) % ways) for i in range(ways)])]
    pallas_call x4 -> x3, Pallas kernels: 5.14 us -> 4.88 us  [call(): pl.pallas_call(kernel, out_shape=out, in_specs=specs, compiler_params=plt...]
  transfers between devices with their start and end apart: 4 -> 1, of which waited for: 1 -> 1; matrix products, arithmetic and copies ran while one was open for 0% -> 0% of each run, Pallas kernels for 13% -> 0%
where the time goes in v2:
time: 44.7 us; the launch traced here: 44.5 us
  blocking collectives  25.4 us (57%)
  Pallas kernels  8.52 us (19%)
  waiting for transfers between devices  6.51 us (15%)
  starting transfers between devices  3.31 us (7%)
  between operations  0.7 us (2%)
    all_to_all x1, blocking collectives, shards(): lax.all_to_all(outgoing, 'ep', split_axis=0, concat_axis=0, tiled=True)  13.1 us
    all_gather x1, blocking collectives, shards(): gathered = lax.all_gather(partial, 'tp')  6.54 us
    all_to_all x1, waiting for transfers between devices, shards(): lax.all_to_all(out, 'ep', split_axis=0, concat_axis=0, tiled=True)  6.51 us
    all_gather x1, blocking collectives, shards(): lax.all_gather(hidden, 'tp')  5.77 us
    pallas_call x3, Pallas kernels, call(): pl.pallas_call(kernel, out_shape=out, in_specs=specs, compiler_params=plt...  4.88 us
    pallas_call x1, Pallas kernels, shards(): pl.pallas_call(mixer_kernel, out_shape=(struct((count, width), F32), stru...  3.39 us
    all_to_all x1, starting transfers between devices, shards(): lax.all_to_all(out, 'ep', split_axis=0, concat_axis=0, tiled=True)  3.31 us
  transfers between devices with their start and end apart: 1, of which 1 were waited for; matrix products, arithmetic and copies ran while one was open for 0% of the time, Pallas kernels for 0%

profile of v2, /device:TPU:0, one launch (start us, length us, event | category | flops | bytes accessed | tf_op | source)
XLA Modules:
  0.0 44.5 jit_solution(1438179411273818963)
XLA Ops:
  0.6 0.0 slice-start
  0.7 3.4 %shard_map.211 = (f32[4,2048]{1,0:T(4,128)S(1)}, f32[64,64]{1,0:T(8,128)}, f32[64,64]{1,0:T(8,128)}, bf16[4,2048]{1,0:T(4,128)(2,1)S(1)}, f32[1,2048]{1,0:T(1,12...) custom-call(s32[1]{0:T(128)} %bitcast.1.base, bf16[4,2048]{1,0:T(4,128)(2,1)} %refs_0_.1, bf16[16,128]{1,0:T(8,128)(2,1)} %bitcast.34, ...), custom_call_target="tpu_custom_call" | custom-call | tf_op jit(solution)/shard_map/pallas_call | solution.py:300
  4.0 6.5 %all-gather.2.gathered = f32[4,4,2048]{2,1,0:T(4,128)S(1)} all-gather(f32[1,4,2048]{2,1,0:T(4,128)S(1)} %bitcast.27), channel_id=2, replica_groups=mesh['ep'=8,'tp'=4] {'tp'}, dimensions={0}, use_global_device_ids=true | all-gather | bytes 163840 | tf_op jit(solution)/shard_map/all_gather | solution.py:316
  10.6 0.0 slice-start.1
  10.6 0.0 copy-start
  10.6 0.0 slice-start.2
  10.6 0.2 shard_map.212
  10.9 13.1 %all_to_all.10.received = bf16[8,2,2048]{2,1,0:T(2,128)(2,1)S(1)} all-to-all(bf16[8,2,2048]{2,1,0:T(2,128)(2,1)S(1)} %get-tuple-element.16), channel_id=1, replica_groups=mesh['ep'=8,'tp'=4] {'ep'}, dimensions={0} | all-to-all | bytes 131072 | tf_op jit(solution)/shard_map/all_to_all | solution.py:333
  24.0 0.0 slice-done
  24.0 0.0 slice-done.1
  24.0 0.0 copy-done
  24.0 0.0 slice-start.3
  24.0 2.3 %shard_map.213 = bf16[16,2048]{1,0:T(8,128)(2,1)S(1)} custom-call(bf16[8,2,2048]{2,1,0:T(2,128)(2,1)S(1)} %all_to_all.10.received, bf16[2048,2048]{1,0:T(8,128)(2,1)S(1)} %bitcast.23, bf16[2048,2048]{1,0:T(8,128)(2,1)S(1)} %copy-done), custom_call_target="tpu_custom_call" | custom-call | tf_op jit(solution)/shard_map/pallas_call | solution.py:238
  26.3 5.8 %all-gather.1 = bf16[64,2048]{1,0:T(8,128)(2,1)S(1)} all-gather(bf16[16,2048]{1,0:T(8,128)(2,1)S(1)} %shard_map.213), channel_id=3, replica_groups=mesh['ep'=8,'tp'=4] {'tp'}, dimensions={0}, use_global_device_ids=true | all-gather | bytes 327680 | tf_op jit(solution)/shard_map/all_gather | solution.py:344
  32.1 0.0 slice-done.2
  32.1 0.0 slice-done.3
  32.1 1.8 %shard_map.214 = bf16[8,2,512]{2,1,0:T(2,128)(2,1)} custom-call(bf16[4,16,2048]{2,1,0:T(8,128)(2,1)S(1)} %bitcast.26, bf16[8192,512]{1,0:T(8,128)(2,1)S(1)} %bitcast.25), custom_call_target="tpu_custom_call" | custom-call | tf_op jit(solution)/shard_map/pallas_call | solution.py:238
  33.9 3.3 %all-to-all-start.1 = ((bf16[8,2,512]{2,1,0:T(2,128)(2,1)}), bf16[8,2,512]{2,1,0:T(2,128)(2,1)S(1)}, u32[]{:S(2)}, u32[]{:S(2)}) async-start(bf16[8,2,512]{2,1,0:T(2,128)(2,1)} %shard_map.214), calls=%async_computation.1 | async-start | bytes 32768 | tf_op jit(solution)/shard_map/all_to_all | solution.py:347
  37.2 6.5 %all-to-all-done.1.returned = bf16[8,2,512]{2,1,0:T(2,128)(2,1)S(1)} async-done(((bf16[8,2,512]{2,1,0:T(2,128)(2,1)}), bf16[8,2,512]{2,1,0:T(2,128)(2,1)S(1)}, u32[]{:S(2)}, u32[]{:S(2)}) %all-to-all-start.1) | async-done | bytes 16416 | tf_op jit(solution)/shard_map/all_to_all | solution.py:347
  43.7 0.8 %shard_map.215 = bf16[4,512]{1,0:T(4,128)(2,1)} custom-call(s32[1]{0:T(128)} %bitcast.start, bf16[8,2,512]{2,1,0:T(2,128)(2,1)S(1)} %all-to-all-done.1.returned, f32[16,4]{1,0:T(8,128)S(1)} %get-tuple-element.17.table, bf16[4,2048]{1,0:T(4,128)(2,1)S(1)} %get-tuple-element.18.hidden), custom_call_target="tpu_custom_call" | custom-call | tf_op jit(solution)/shard_map/pallas_call | solution.py:238
  (2 shorter events, 0.0 us)
Async XLA Ops:
  0.6 23.3 %slice-start = ((s8[8388608]{0:T(1024)(128)(4,1)}), s8[4194304]{0:T(1024)(128)(4,1)S(1)}, s32[]{:S(2)}) async-start(s8[8388608]{0:T(1024)(128)(4,1)} %bitcast.22), calls=%async_computation.2 | async-start | bytes 8388608
  10.6 13.4 %slice-start.1 = ((s8[8388608]{0:T(1024)(128)(4,1)}), s8[4194304]{0:T(1024)(128)(4,1)S(1)}, s32[]{:S(2)}) async-start(s8[8388608]{0:T(1024)(128)(4,1)} %bitcast.22), calls=%async_computation.3 | async-start | bytes 8388608
  10.6 13.4 %copy-start = (bf16[2048,2048]{1,0:T(8,128)(2,1)S(1)}, bf16[2048,2048]{1,0:T(8,128)(2,1)}, u32[]{:S(2)}) copy-start(bf16[2048,2048]{1,0:T(8,128)(2,1)} %up.3) | copy-start | bytes 25165828
  10.6 21.5 %slice-start.2 = ((s8[8388608]{0:T(1024)(128)(4,1)}), s8[4194304]{0:T(1024)(128)(4,1)S(1)}, s32[]{:S(2)}) async-start(s8[8388608]{0:T(1024)(128)(4,1)} %bitcast.24), calls=%async_computation.4 | async-start | bytes 8388608
  24.0 8.1 %slice-start.3 = ((s8[8388608]{0:T(1024)(128)(4,1)}), s8[4194304]{0:T(1024)(128)(4,1)S(1)}, s32[]{:S(2)}) async-start(s8[8388608]{0:T(1024)(128)(4,1)} %bitcast.24), calls=%async_computation.5 | async-start | bytes 8388608
  33.9 9.8 %all-to-all-start.1 = ((bf16[8,2,512]{2,1,0:T(2,128)(2,1)}), bf16[8,2,512]{2,1,0:T(2,128)(2,1)S(1)}, u32[]{:S(2)}, u32[]{:S(2)}) async-start(bf16[8,2,512]{2,1,0:T(2,128)(2,1)} %shard_map.214), calls=%async_computation.1 | async-start | bytes 32768 | tf_op jit(solution)/shard_map/all_to_all | solution.py:347
